TPU v7x, 128 devices: a whole 4x4x4 slice. The times are simulated.
128 devices in a mesh: rep: 2 (over z_hi), fs: 32 (over z_lo, y, x), tp: 2 (over core).
Axes of the slice: x: 4, y: 4, z: 4 (z_hi: 2, z_lo: 2; z = z_hi * 2 + z_lo), core: 2. Of those that a mesh axis runs over, the one named last changes fastest.
Arguments:
- resid: bfloat16 [49152, 2048], P(('rep', 'fs', 'tp')), may hold values from -6 to 6
- mix_gain: float32 [2048], replicated, may hold values from 0.1 to 1.9
- query_weight: bfloat16 [2048, 1024], P('fs', 'tp'), may hold values from -0.125 to 0.125
- key_weight: bfloat16 [2048, 1024], P('fs', 'tp'), may hold values from -0.125 to 0.125
- value_weight: bfloat16 [2048, 2048], P('fs', 'tp'), may hold values from -0.125 to 0.125
- head_gain: float32 [2048], P('tp'), may hold values from 0.1 to 1.9
- out_weight: bfloat16 [2048, 2048], P('tp', 'fs'), may hold values from -0.125 to 0.125
- mlp_gain: float32 [2048], replicated, may hold values from 0.1 to 1.9
- gate_weight: bfloat16 [2048, 2816], P('fs', 'tp'), may hold values from -0.125 to 0.125
- up_weight: bfloat16 [2048, 2816], P('fs', 'tp'), may hold values from -0.125 to 0.125
- down_weight: bfloat16 [2816, 2048], P('tp', 'fs'), may hold values from -0.109375 to 0.109375
Outputs:
- layer_out: bfloat16 [49152, 2048], P(('rep', 'fs', 'tp'))
All inputs are finite; a program needn't handle non-finite values.
Results may differ from a plain program's by a relative error of at most 0.014.
Values may be sent and summed in bfloat16 or wider, within the bound.
No kernel may reach another device: no remote copies, remote signals or barrier semaphores. Data moves between devices by JAX's collectives and lax.ppermute only.
A program may use at most 128 MiB of HBM per device.

v0:
```python
import jax
import jax.numpy as jnp
from jax import lax
from jax.sharding import Mesh
from jax.sharding import PartitionSpec as P

DK = 256
DV = 512
BLOCK = 128
FS = ("fs_0", "fs_1", "fs_2")
REP_FS_TP = ("rep", "fs_0", "fs_1", "fs_2", "tp")


norm_eps = 1e-06
rope_base = 10000.0


def cut_along(shard, dim, peers):
    lengths = shard.shape
    pieces = shard.reshape(*lengths[:dim], peers, lengths[dim] // peers, *lengths[dim + 1 :])
    return jnp.moveaxis(pieces, dim, 0)


def sum_at_owner(shard, axis, dim):
    pieces = cut_along(shard, dim, lax.axis_size(axis))
    arrived = lax.all_to_all(pieces, axis, split_axis=0, concat_axis=0, tiled=True)
    return arrived.astype(jnp.float32).sum(axis=0)


def laid_out(pieces, dim):
    pieces = jnp.moveaxis(pieces, 0, dim)
    lengths = pieces.shape
    return pieces.reshape(*lengths[:dim], lengths[dim] * lengths[dim + 1], *lengths[dim + 2 :])


def stacked_from(shard, axes, order):
    pieces = shard
    for k in order:
        pieces = lax.all_gather(pieces, axes[k])
    done = order[::-1]
    back = [done.index(k) for k in range(len(axes))]
    pieces = pieces.transpose(*back, *range(len(axes), pieces.ndim))
    return pieces.reshape(-1, *shard.shape)


def whole_of(shard, axes, order, dim):
    return laid_out(stacked_from(shard, axes, order), dim)


def rms_scale(values, gain):
    widened = values.astype(jnp.float32)
    scaled = widened * lax.rsqrt(jnp.mean(widened * widened, axis=-1, keepdims=True) + norm_eps)
    return (scaled * gain).astype(jnp.bfloat16)


def rotate(vectors):
    length_total = vectors.shape[0]
    half_width = vectors.shape[-1] // 2
    position = jnp.arange(length_total, dtype=jnp.float32)
    inverse = 1.0 / rope_base ** jnp.linspace(0.0, 1.0, half_width, dtype=jnp.float32)
    angle = position[:, None] * inverse[None, :]
    cosine = jnp.cos(angle)[:, None, :]
    sine = jnp.sin(angle)[:, None, :]
    first = vectors[..., :half_width]
    second = vectors[..., half_width:]
    return jnp.concatenate(
        [first * cosine - second * sine, second * cosine + first * sine], axis=-1
    )


def decay_tables(head_ids, block):
    log_gamma = jnp.log1p(-(2.0 ** (-5.0 - 2.0 * head_ids.astype(jnp.float32))))
    offset = jnp.arange(block, dtype=jnp.float32)
    distance = offset[:, None] - offset[None, :]
    inside = jnp.where(
        distance >= 0, jnp.exp(log_gamma[:, None, None] * jnp.maximum(distance, 0.0)), 0.0
    )
    query_decay = jnp.exp(log_gamma[:, None] * (offset + 1.0))
    key_decay = jnp.exp(log_gamma[:, None] * (block - 1.0 - offset))
    block_decay = jnp.exp(log_gamma * block)
    return (inside, query_decay, key_decay, block_decay)


def retain(queries, keys, values, head_ids, block):
    length_total, heads, key_width = queries.shape
    value_width = values.shape[-1]
    count = length_total // block
    inside, query_decay, key_decay, block_decay = decay_tables(head_ids, block)

    def blocks(tensor):
        return tensor.reshape(count, block, heads, tensor.shape[-1]).transpose(0, 2, 1, 3)

    def advance(memory, inputs):
        query_tile_rows, key_tile_rows, value_block = inputs
        attention_scores = jnp.einsum(
            "zvf,zjf->zvj", query_tile_rows, key_tile_rows, preferred_element_type=jnp.float32
        )
        weights = (attention_scores * inside).astype(jnp.bfloat16)
        within = jnp.einsum(
            "hlm,hmv->hlv", weights, value_block, preferred_element_type=jnp.float32
        )
        carried = (
            jnp.einsum(
                "hld,hdv->hlv",
                query_tile_rows,
                memory.astype(jnp.bfloat16),
                preferred_element_type=jnp.float32,
            )
            * query_decay[:, :, None]
        )
        weighted_keys = (key_tile_rows.astype(jnp.float32) * key_decay[:, :, None]).astype(
            jnp.bfloat16
        )
        memory = memory * block_decay[:, None, None] + jnp.einsum(
            "hld,hlv->hdv", weighted_keys, value_block, preferred_element_type=jnp.float32
        )
        return (memory, within + carried)

    start_state = jnp.zeros((heads, key_width, value_width), jnp.float32)
    _, outputs = lax.scan(advance, start_state, (blocks(queries), blocks(keys), blocks(values)))
    return outputs.transpose(0, 2, 1, 3).reshape(length_total, heads, value_width)


def head_scale(retained, gain):
    scaled = retained * lax.rsqrt(jnp.mean(retained * retained, axis=-1, keepdims=True) + norm_eps)
    return (scaled.reshape(retained.shape[0], -1) * gain).astype(jnp.bfloat16)


def shards(
    resid,
    mix_gain,
    query_weight,
    key_weight,
    value_weight,
    head_gain,
    out_weight,
    mlp_gain,
    gate_weight,
    up_weight,
    down_weight,
):
    token_rows = resid.shape[0]
    length_total = token_rows * lax.axis_size("tp")
    key_cols = query_weight.shape[1]
    heads_here = key_cols // DK
    normed = rms_scale(resid, mix_gain)
    mixer_shard = jnp.concatenate([query_weight, key_weight, value_weight], axis=1)
    mixer_full = lax.all_gather(mixer_shard, FS, axis=0, tiled=True)
    projected = jnp.dot(
        lax.all_gather(normed, "tp", axis=0, tiled=True),
        mixer_full,
        preferred_element_type=jnp.float32,
    ).astype(jnp.bfloat16)
    queries = projected[:, :key_cols].astype(jnp.float32).reshape(length_total, heads_here, DK)
    keys = (
        projected[:, key_cols : 2 * key_cols]
        .astype(jnp.float32)
        .reshape(length_total, heads_here, DK)
    )
    values = projected[:, 2 * key_cols :].reshape(length_total, heads_here, DV)
    query_rot = rotate(queries).astype(jnp.bfloat16)
    key_rot = (rotate(keys) * DK ** (-0.5)).astype(jnp.bfloat16)
    head_ids = lax.axis_index("tp") * heads_here + jnp.arange(heads_here, dtype=jnp.int32)
    retained = retain(query_rot, key_rot, values, head_ids, BLOCK)
    head_out = head_scale(retained, head_gain)
    out_full = lax.all_gather(out_weight, FS, axis=1, tiled=True)
    selected = head_out
    mixer_sum = sum_at_owner(
        jnp.dot(selected, out_full, preferred_element_type=jnp.float32).astype(jnp.bfloat16),
        "tp",
        0,
    )
    middle = (resid.astype(jnp.float32) + mixer_sum).astype(jnp.bfloat16)
    normed_mlp = rms_scale(middle, mlp_gain)
    local_units = gate_weight.shape[1]
    mlp_shard = jnp.concatenate([gate_weight, up_weight], axis=1)
    mlp_full = lax.all_gather(mlp_shard, FS, axis=0, tiled=True)
    both = jnp.dot(
        lax.all_gather(normed_mlp, "tp", axis=0, tiled=True),
        mlp_full,
        preferred_element_type=jnp.float32,
    )
    hidden_units = (jax.nn.silu(both[:, :local_units]) * both[:, local_units:]).astype(jnp.bfloat16)
    down_full = whole_of(down_weight, FS, (0, 1, 2), 1)
    selected = hidden_units
    mlp_sum = sum_at_owner(
        jnp.dot(selected, down_full, preferred_element_type=jnp.float32).astype(jnp.bfloat16),
        "tp",
        0,
    )
    return (middle.astype(jnp.float32) + mlp_sum).astype(jnp.bfloat16)


def solution(mesh):
    torus = Mesh(
        mesh.devices.reshape(mesh.shape["rep"], 2, 4, 4, mesh.shape["tp"]),
        ("rep", "fs_0", "fs_1", "fs_2", "tp"),
    )
    return jax.shard_map(
        shards,
        mesh=torus,
        in_specs=(
            P(REP_FS_TP, None),
            P(),
            P(FS, "tp"),
            P(FS, "tp"),
            P(FS, "tp"),
            P("tp"),
            P("tp", FS),
            P(),
            P(FS, "tp"),
            P(FS, "tp"),
            P("tp", FS),
        ),
        out_specs=P(REP_FS_TP, None),
        check_vma=False,
    )
```

profile of v0, /device:TPU:1, one launch (start us, length us, event | category | flops | bytes accessed | tf_op | source)
XLA Modules:
  0.0 678.0 jit_solution(7657517100570402122)
XLA Ops:
  6.5 7.8 %all-gather = bf16[2816,64]{0,1:T(8,128)(2,1)S(1)} all-gather(bf16[1408,64]{0,1:T(8,128)(2,1)} %param.25), channel_id=2, replica_groups=mesh['rep'=2,'fs_0'=2,'fs_1'=4,'fs_2'=4,'tp'=2] {'fs_0'}, dimensions={0}, use_global_device_ids=true | all-gather | bytes 540672 | tf_op jit(solution)/shard_map/all_gather | solution.py:39
  15.2 1.8 fusion.44
  17.0 1.6 fusion.46
  20.3 2.2 fusion.58
  22.5 20.7 %all-gather.21.cloned.1.call-done = bf16[8,1408,64]{1,2,0:T(8,128)(2,1)} async-done(((bf16[2,1408,64]{1,2,0:T(8,128)(2,1)}), bf16[8,1408,64]{1,2,0:T(8,128)(2,1)}) %all-gather.21.cloned.1.call-update) | async-done | bytes 1441808 | tf_op jit(solution)/shard_map/all_gather | solution.py:39
  43.3 17.4 %all-gather.11.cloned.1.call-done = bf16[768,2048]{1,0:T(8,128)(2,1)} async-done(((bf16[384,2048]{1,0:T(8,128)(2,1)}), bf16[768,2048]{1,0:T(8,128)(2,1)}) %all-gather.11.cloned.1.call-update) | async-done | bytes 3145744 | tf_op jit(solution)/shard_map/all_gather | solution.py:150
  60.7 148.5 %all-gather.13.cloned.1.call-done = bf16[2048,2048]{1,0:T(8,128)(2,1)} async-done(((bf16[64,2048]{1,0:T(8,128)(2,1)}), bf16[2048,2048]{1,0:T(8,128)(2,1)}) %all-gather.13.cloned.1.call-update) | async-done | bytes 8388624 | tf_op jit(solution)/shard_map/all_gather | solution.py:148
  209.2 10.0 %convolution_convert_fusion = bf16[768,2048]{1,0:T(8,128)(2,1)S(1)} fusion(bf16[768,2048]{1,0:T(8,128)(2,1)} %all-gather.11.cloned.1.call-done, bf16[2048,2048]{1,0:T(8,128)(2,1)} %all-gather.13.cloned.1.call-done), kind=kOutput, calls=%fused_computation.53 | convolution fusion | flops 6444023808 | bytes 14680064 | tf_op jit(solution)/shard_map/dot_general | solution.py:149
  219.2 2.1 slice_convert_fusion
  221.3 1.3 slice.39
  222.7 3.1 reshape.166
  225.7 3.1 reshape.168
  228.8 3.8 reshape_reshape.3
  232.6 3.0 copy.74
  239.2 30.2 %while.15 = (s32[]{:T(128)}, f32[2,256,512]{2,1,0:T(8,128)S(1)}, f32[6,2,128,512]{3,2,1,0:T(8,128)}, bf16[6,2,128,256]{3,2,0,1:T(8,128)(2,1)}, bf16[6,2,128,512]...) while((s32[]{:T(128)}, f32[2,256,512]{2,1,0:T(8,128)S(1)}, ...), condition=%wide.region_2.4_spmd.clone.clone.clone, body=%wide.region_1.3_spmd.clone.clone.clone.sunk | while | flops 186188304 | bytes 5857972 | solution.py:120
  240.4 2.3 fusion.84
  242.8 1.5 convolution_add_fusion.3
  244.4 1.1 convolution_multiply_fusion.3
  245.5 2.2 fusion.84
  247.8 1.5 convolution_add_fusion.3
  249.4 1.1 convolution_multiply_fusion.3
  250.5 2.2 fusion.84
  252.8 1.5 convolution_add_fusion.3
  255.6 2.3 fusion.84
  257.9 1.5 convolution_add_fusion.3
  259.5 1.1 convolution_multiply_fusion.3
  260.6 2.3 fusion.84
  262.9 1.5 convolution_add_fusion.3
  264.5 1.1 convolution_multiply_fusion.3
  265.7 2.2 fusion.84
  267.9 1.5 convolution_add_fusion.3
  269.5 2.2 multiply_reduce_fusion
  271.8 1.2 mul.286
  273.1 2.4 copy.63
  275.5 2.4 copy.50
  277.9 2.4 copy.62
  280.3 87.4 %all-gather.15.cloned.1.call-done = bf16[1024,2048]{0,1:T(8,128)(2,1)} async-done(((bf16[1024,64]{0,1:T(8,128)(2,1)}), bf16[1024,2048]{0,1:T(8,128)(2,1)}) %all-gather.15.cloned.1.call-update) | async-done | bytes 4194320 | tf_op jit(solution)/shard_map/all_gather | solution.py:166
  367.7 7.5 %convolution_convert_fusion.1 = bf16[768,2048]{1,0:T(8,128)(2,1)S(1)} fusion(bf16[1024,2048]{0,1:T(8,128)(2,1)} %all-gather.15.cloned.1.call-done, f32[768,1024]{1,0:T(8,128)} %bitcast.90, f32[768,1024]{1,0:T(8,128)} %bitcast.89, f32[1024]{0:T(1024)S(1)} %copy-done.13), kind=kOutput, calls=%fused_computation.54 | convolution fusion | flops 3225157632 | bytes 13635584 | tf_op jit(solution)/shard_map/dot_general | solution.py:169
  375.2 27.1 %all_to_all.10 = bf16[2,384,2048]{2,1,0:T(8,128)(2,1)S(1)} all-to-all(bf16[2,384,2048]{2,1,0:T(8,128)(2,1)S(1)} %bitcast.91), channel_id=1, replica_groups=mesh['rep'=2,'fs_0'=2,'fs_1'=4,'fs_2'=4,'tp'=2] {'tp'}, dimensions={0} | all-to-all | bytes 6291456 | tf_op jit(solution)/shard_map/all_to_all | solution.py:26
  403.7 1.6 fusion.50
  406.2 44.7 %all-gather.23.cloned.1.call-done = bf16[16,2,1408,64]{2,3,1,0:T(8,128)(2,1)} async-done(((bf16[4,2,1408,64]{2,3,1,0:T(8,128)(2,1)}), bf16[16,2,1408,64]{2,3,1,0:T(8,128)(2,1)}) %all-gather.23.cloned.1.call-update) | async-done | bytes 5767184 | tf_op jit(solution)/shard_map/all_gather | solution.py:39
  450.9 5.7 copy.53
  456.5 11.9 %all-gather.17.cloned.1.call-done = bf16[768,2048]{1,0:T(8,128)(2,1)} async-done(((bf16[384,2048]{1,0:T(8,128)(2,1)}), bf16[768,2048]{1,0:T(8,128)(2,1)}) %all-gather.17.cloned.1.call-update) | async-done | bytes 3145744 | tf_op jit(solution)/shard_map/all_gather | solution.py:179
  468.4 155.2 %all-gather.19.cloned.1.call-done = bf16[2048,2816]{1,0:T(8,128)(2,1)} async-done(((bf16[64,2816]{1,0:T(8,128)(2,1)}), bf16[2048,2816]{1,0:T(8,128)(2,1)}) %all-gather.19.cloned.1.call-update) | async-done | bytes 11534352 | tf_op jit(solution)/shard_map/all_gather | solution.py:177
  623.6 13.8 %fusion.66 = f32[768,2816]{1,0:T(8,128)S(1)} fusion(bf16[768,2048]{1,0:T(8,128)(2,1)} %all-gather.17.cloned.1.call-done, bf16[2048,2816]{1,0:T(8,128)(2,1)} %all-gather.19.cloned.1.call-done), kind=kOutput, calls=%fused_computation.100 | convolution fusion | flops 8858370048 | bytes 23330816 | tf_op jit(solution)/shard_map/dot_general | solution.py:178
  637.5 5.3 convolution_convert_fusion.2
  642.8 26.0 %all_to_all.11 = bf16[2,384,2048]{2,1,0:T(8,128)(2,1)S(1)} all-to-all(bf16[2,384,2048]{2,1,0:T(8,128)(2,1)S(1)} %bitcast.92), channel_id=1, replica_groups=mesh['rep'=2,'fs_0'=2,'fs_1'=4,'fs_2'=4,'tp'=2] {'tp'}, dimensions={0} | all-to-all | bytes 6291456 | tf_op jit(solution)/shard_map/all_to_all | solution.py:26
  669.5 1.6 fusion.51
  (78 shorter events, 12.1 us)
Async XLA Ops:
  6.5 10.5 %copy-start = (bf16[384,2048]{1,0:T(8,128)(2,1)S(1)}, bf16[384,2048]{1,0:T(8,128)(2,1)}, u32[]{:S(2)}) copy-start(bf16[384,2048]{1,0:T(8,128)(2,1)} %param.15) | copy-start | bytes 4718596
  6.5 10.5 %copy-start.11 = (f32[2048]{0:T(1024)S(1)}, f32[2048]{0:T(1024)}, u32[]{:S(2)}) copy-start(f32[2048]{0:T(1024)} %param.16) | copy-start | bytes 24580
  6.5 36.7 %all-gather.21.cloned.1.call-start = ((), (), s32[]{:S(2)}) async-start(), calls=%async_computation.7 | async-start | bytes 1802240 | tf_op jit(solution)/shard_map/all_gather | solution.py:39
  15.1 3.6 copy-start.8
  15.1 3.6 copy-start.9
  15.1 3.6 copy-start.10
  15.1 45.5 %all-gather.11.cloned.1.call-start = ((), (), s32[]{:S(2)}) async-start(), calls=%async_computation.2 | async-start | bytes 4718592 | tf_op jit(solution)/shard_map/all_gather | solution.py:150
  18.6 190.5 %all-gather.13.cloned.1.call-start = ((), (), s32[]{:S(2)}) async-start(), calls=%async_computation.3 | async-start | bytes 8650752 | tf_op jit(solution)/shard_map/all_gather | solution.py:148
  19.5 348.2 %all-gather.15.cloned.1.call-start = ((), (), s32[]{:S(2)}) async-start(), calls=%async_computation.4 | async-start | bytes 4325376 | tf_op jit(solution)/shard_map/all_gather | solution.py:166
  20.1 430.8 %all-gather.23.cloned.1.call-start = ((), (), s32[]{:S(2)}) async-start(), calls=%async_computation.8 | async-start | bytes 7208960 | tf_op jit(solution)/shard_map/all_gather | solution.py:39
  43.2 425.2 %all-gather.17.cloned.1.call-start = ((), (), s32[]{:S(2)}) async-start(), calls=%async_computation.5 | async-start | bytes 4718592 | tf_op jit(solution)/shard_map/all_gather | solution.py:179
  232.6 3.0 copy-start.2
  232.6 3.0 copy-start.3
  235.6 1.1 copy-start.5
  273.1 2.4 copy-start.1
  277.9 89.8 %copy-start.13 = (f32[1024]{0:T(1024)S(1)}, f32[1024]{0:T(1024)}, u32[]{:S(2)}) copy-start(f32[1024]{0:T(1024)} %param.20) | copy-start | bytes 12292
  403.0 0.7 copy-start.12
  403.6 1.8 copy-start.6
  403.6 1.8 copy-start.7
  405.3 218.3 %all-gather.19.cloned.1.call-start = ((), (), s32[]{:S(2)}) async-start(), calls=%async_computation.6 | async-start | bytes 11894784 | tf_op jit(solution)/shard_map/all_gather | solution.py:177
  623.6 13.8 %copy-start.4 = (bf16[2,4,4,1408,64]{3,4,2,1,0:T(8,128)(2,1)S(1)}, bf16[2,4,4,1408,64]{3,4,2,1,0:T(8,128)(2,1)}, u32[]{:S(2)}) copy-start(bf16[2,4,4,1408,64]{3,4,2,1,0:T(8,128)(2,1)} %copy.53) | copy-start | bytes 17301508
Sparse Core Ops, SparseCore 0:
  15.2 27.9 all-gather.20
  44.9 15.7 all-gather.10
  62.3 146.7 all-gather.12
  210.7 157.0 all-gather.14
  369.2 81.5 all-gather.22
  452.4 15.9 all-gather.16
  470.0 153.5 all-gather.18
where the time goes:
time: 679 us; the launch traced here: 678 us
  waiting for transfers between devices  486 us (72%)
  matrix products  66.2 us (10%)
  blocking collectives  60.8 us (9%)
  local copies, waits for them, and re-layouts  30.7 us (5%)
  other arithmetic  19.8 us (3%)
  between operations  13.8 us (2%)
    all_gather x1, waiting for transfers between devices, shards(): mlp_full = lax.all_gather(mlp_shard, FS, axis=0, tiled=True)  155 us
    all_gather x1, waiting for transfers between devices, shards(): mixer_full = lax.all_gather(mixer_shard, FS, axis=0, tiled=True)  148 us
    all_gather x1, waiting for transfers between devices, shards(): out_full = lax.all_gather(out_weight, FS, axis=1, tiled=True)  87.4 us
    all_gather x2, waiting for transfers between devices, stacked_from(): pieces = lax.all_gather(pieces, axes[k])  65.4 us
    all_to_all x2, blocking collectives, sum_at_owner(): lax.all_to_all(pieces, axis, split_axis=0, concat_axis=0, tiled=True)  53 us
    all_gather x1, waiting for transfers between devices, shards(): lax.all_gather(normed, 'tp', axis=0, tiled=True)  17.4 us
    dot_general x1, matrix products, shards(): jnp.dot(lax.all_gather(normed_mlp, 'tp', axis=0, tiled=True), mlp_full, p...  13.8 us
    dot_general x6, matrix products, advance(): jnp.einsum('hlm,hmv->hlv', weights, value_block, preferred_element_type=j...  13.6 us
  transfers between devices with their start and end apart: 7, of which 7 were waited for; matrix products, arithmetic and copies ran while one was open for 14% of the time, Pallas kernels for 0%

commit v1 on v0

--- a/solution.py
+++ b/solution.py
@@ -15,36 +15,26 @@
 rope_base = 10000.0
 
 
-def cut_along(shard, dim, peers):
-    lengths = shard.shape
-    pieces = shard.reshape(*lengths[:dim], peers, lengths[dim] // peers, *lengths[dim + 1 :])
-    return jnp.moveaxis(pieces, dim, 0)
-
-
-def sum_at_owner(shard, axis, dim):
-    pieces = cut_along(shard, dim, lax.axis_size(axis))
-    arrived = lax.all_to_all(pieces, axis, split_axis=0, concat_axis=0, tiled=True)
-    return arrived.astype(jnp.float32).sum(axis=0)
-
-
-def laid_out(pieces, dim):
-    pieces = jnp.moveaxis(pieces, 0, dim)
-    lengths = pieces.shape
-    return pieces.reshape(*lengths[:dim], lengths[dim] * lengths[dim + 1], *lengths[dim + 2 :])
-
-
-def stacked_from(shard, axes, order):
-    pieces = shard
-    for k in order:
-        pieces = lax.all_gather(pieces, axes[k])
-    done = order[::-1]
-    back = [done.index(k) for k in range(len(axes))]
-    pieces = pieces.transpose(*back, *range(len(axes), pieces.ndim))
-    return pieces.reshape(-1, *shard.shape)
-
-
-def whole_of(shard, axes, order, dim):
-    return laid_out(stacked_from(shard, axes, order), dim)
+TORUS = ("rep", "fs_0", "fs_1", "fs_2")
+
+
+def with_partner(shard):
+    other = lax.ppermute(shard, "tp", ((0, 1), (1, 0)))
+    first = lax.axis_index("tp") == 0
+    return jnp.concatenate([jnp.where(first, shard, other), jnp.where(first, other, shard)], axis=0)
+
+
+def sum_at_owner(partial):
+    rows = partial.shape[0] // 2
+    index = lax.axis_index("tp")
+    mine = lax.dynamic_slice_in_dim(partial, index * rows, rows, 0)
+    away = lax.dynamic_slice_in_dim(partial, (1 - index) * rows, rows, 0)
+    arrived = lax.ppermute(away, "tp", ((0, 1), (1, 0)))
+    return mine.astype(jnp.float32) + arrived.astype(jnp.float32)
+
+
+def half_of(first, second):
+    return jnp.where(lax.axis_index("rep") == 0, first, second)
 
 
 def rms_scale(values, gain):
@@ -143,50 +133,57 @@
     length_total = token_rows * lax.axis_size("tp")
     key_cols = query_weight.shape[1]
     heads_here = key_cols // DK
-    normed = rms_scale(resid, mix_gain)
-    mixer_shard = jnp.concatenate([query_weight, key_weight, value_weight], axis=1)
-    mixer_full = lax.all_gather(mixer_shard, FS, axis=0, tiled=True)
-    projected = jnp.dot(
-        lax.all_gather(normed, "tp", axis=0, tiled=True),
-        mixer_full,
-        preferred_element_type=jnp.float32,
-    ).astype(jnp.bfloat16)
-    queries = projected[:, :key_cols].astype(jnp.float32).reshape(length_total, heads_here, DK)
-    keys = (
-        projected[:, key_cols : 2 * key_cols]
-        .astype(jnp.float32)
-        .reshape(length_total, heads_here, DK)
-    )
-    values = projected[:, 2 * key_cols :].reshape(length_total, heads_here, DV)
+    out_shard = out_weight.T
+    down_shard = down_weight.T
+    half_out = out_shard.shape[1] // 2
+    half_down = down_shard.shape[1] // 2
+    first_shard = half_of(
+        jnp.concatenate([query_weight, key_weight, out_shard[:, :half_out]], axis=1),
+        jnp.concatenate([value_weight, out_shard[:, half_out:]], axis=1),
+    )
+    second_shard = half_of(
+        jnp.concatenate([gate_weight, down_shard[:, :half_down]], axis=1),
+        jnp.concatenate([up_weight, down_shard[:, half_down:]], axis=1),
+    )
+    first_full = lax.all_gather(first_shard, TORUS, axis=0, tiled=True)
+    first_full, second_shard = lax.optimization_barrier((first_full, second_shard))
+    second_full = lax.all_gather(second_shard, TORUS, axis=0, tiled=True)
+    width = first_full.shape[0] // 2
+
+    def dot(a, b):
+        return jnp.dot(a, b, preferred_element_type=jnp.float32)
+
+    def dot_t(a, b):
+        return lax.dot_general(a, b, (((1,), (1,)), ((), ())), preferred_element_type=jnp.float32)
+
+    normed = with_partner(rms_scale(resid, mix_gain))
+    qk = dot(normed, first_full[:width, : 2 * key_cols]).astype(jnp.bfloat16).astype(jnp.float32)
+    queries = qk[:, :key_cols].reshape(length_total, heads_here, DK)
+    keys = qk[:, key_cols:].reshape(length_total, heads_here, DK)
+    values = dot(normed, first_full[width:, : 2 * key_cols]).astype(jnp.bfloat16)
+    values = values.reshape(length_total, heads_here, DV)
     query_rot = rotate(queries).astype(jnp.bfloat16)
     key_rot = (rotate(keys) * DK ** (-0.5)).astype(jnp.bfloat16)
     head_ids = lax.axis_index("tp") * heads_here + jnp.arange(heads_here, dtype=jnp.int32)
     retained = retain(query_rot, key_rot, values, head_ids, BLOCK)
     head_out = head_scale(retained, head_gain)
-    out_full = lax.all_gather(out_weight, FS, axis=1, tiled=True)
-    selected = head_out
     mixer_sum = sum_at_owner(
-        jnp.dot(selected, out_full, preferred_element_type=jnp.float32).astype(jnp.bfloat16),
-        "tp",
-        0,
+        (
+            dot_t(head_out[:, :half_out], first_full[:width, 2 * key_cols :])
+            + dot_t(head_out[:, half_out:], first_full[width:, 2 * key_cols :])
+        ).astype(jnp.bfloat16)
     )
     middle = (resid.astype(jnp.float32) + mixer_sum).astype(jnp.bfloat16)
-    normed_mlp = rms_scale(middle, mlp_gain)
-    local_units = gate_weight.shape[1]
-    mlp_shard = jnp.concatenate([gate_weight, up_weight], axis=1)
-    mlp_full = lax.all_gather(mlp_shard, FS, axis=0, tiled=True)
-    both = jnp.dot(
-        lax.all_gather(normed_mlp, "tp", axis=0, tiled=True),
-        mlp_full,
-        preferred_element_type=jnp.float32,
-    )
-    hidden_units = (jax.nn.silu(both[:, :local_units]) * both[:, local_units:]).astype(jnp.bfloat16)
-    down_full = whole_of(down_weight, FS, (0, 1, 2), 1)
-    selected = hidden_units
+    normed_mlp = with_partner(rms_scale(middle, mlp_gain))
+    units = gate_weight.shape[1]
+    gate = dot(normed_mlp, second_full[:width, :units])
+    up = dot(normed_mlp, second_full[width:, :units])
+    hidden_units = (jax.nn.silu(gate) * up).astype(jnp.bfloat16)
     mlp_sum = sum_at_owner(
-        jnp.dot(selected, down_full, preferred_element_type=jnp.float32).astype(jnp.bfloat16),
-        "tp",
-        0,
+        (
+            dot_t(hidden_units[:, :half_down], second_full[:width, units:])
+            + dot_t(hidden_units[:, half_down:], second_full[width:, units:])
+        ).astype(jnp.bfloat16)
     )
     return (middle.astype(jnp.float32) + mlp_sum).astype(jnp.bfloat16)
 

time: 679 us -> 254 us (0.37)
  waiting for transfers between devices: 486 us -> 109 us
  blocking collectives: 60.8 us -> 0 us
  matrix products: 66.2 us -> 77.9 us
    all_gather x7 -> x2, waiting for transfers between devices: 486 us -> 98.3 us  [the longest x1 91.9 us: shards(): first_full = lax.all_gather(first_shard, TORUS, axis=0, tiled=True)]
    all_to_all x2 -> x0, blocking collectives: 53 us -> none  [sum_at_owner(): lax.all_to_all(pieces, axis, split_axis=0, concat_axis=0, tiled=True)]
    dot_general x4 -> x8, matrix products: 36.7 us -> 48.1 us  [the longest x4 31.6 us: dot(): return jnp.dot(a, b, preferred_element_type=jnp.float32)]
    ppermute x0 -> x4, waiting for transfers between devices: none -> 10.3 us  [the longest x2 6.2 us: sum_at_owner(): arrived = lax.ppermute(away, 'tp', ((0, 1), (1, 0)))]
    select_n x0 -> x4, other arithmetic: none -> 8.14 us  [the longest x2 4.63 us: with_partner(): jnp.where(first, shard, other)]
    all_gather x1 -> x0, blocking collectives: 7.76 us -> none  [stacked_from(): pieces = lax.all_gather(pieces, axes[k])]
  transfers between devices with their start and end apart: 7 -> 6, of which waited for: 7 -> 6; matrix products, arithmetic and copies ran while one was open for 14% -> 37% of each run, Pallas kernels for 0% -> 0%
where the time goes in v1:
time: 254 us
  waiting for transfers between devices  109 us (43%)
  matrix products  77.9 us (31%)
  local copies, waits for them, and re-layouts  26.6 us (10%)
  other arithmetic  23.9 us (9%)
  between operations  13.7 us (5%)
  starting transfers between devices  2.71 us (1%)
    all_gather x1, waiting for transfers between devices, shards(): first_full = lax.all_gather(first_shard, TORUS, axis=0, tiled=True)  91.9 us
    dot_general x4, matrix products, dot(): return jnp.dot(a, b, preferred_element_type=jnp.float32)  31.6 us
    dot_general x4, matrix products, dot_t(): lax.dot_general(a, b, (((1,), (1,)), ((), ())), preferred_element_type=jn...  16.5 us
    dot_general x6, matrix products, advance(): jnp.einsum('hlm,hmv->hlv', weights, value_block, preferred_element_type=j...  13.8 us
    dot_general x6, matrix products, advance(): jnp.einsum('hld,hlv->hdv', weighted_keys, value_block, preferred_element_...  9.12 us
    dot_general x6, matrix products, advance(): jnp.einsum('hld,hdv->hlv', query_tile_rows, memory.astype(jnp.bfloat16),...  6.89 us
    another operation x2, local copies, waits for them, and re-layouts, blocks(): tensor.reshape(count, block, heads, tensor.shape[-1]).transpose(0, 2, 1, 3)  6.82 us
    all_gather x1, waiting for transfers between devices, shards(): second_full = lax.all_gather(second_shard, TORUS, axis=0, tiled=True)  6.4 us
  transfers between devices with their start and end apart: 6, of which 6 were waited for; matrix products, arithmetic and copies ran while one was open for 37% of the time, Pallas kernels for 0%

profile of v1, /device:TPU:1, one launch (start us, length us, event | category | flops | bytes accessed | tf_op | source)
XLA Modules:
  0.0 253.6 jit_solution(15682276465543523152)
XLA Ops:
  7.5 1.7 maximum_select_fusion.1
  10.4 1.8 maximum_select_fusion
  12.2 91.9 %all-gather.3.cloned.1.call-done = bf16[4096,1536]{1,0:T(8,128)(2,1)} async-done(((bf16[64,1536]{1,0:T(8,128)(2,1)}), bf16[4096,1536]{1,0:T(8,128)(2,1)}) %all-gather.3.cloned.1.call-update) | async-done | bytes 12582928 | tf_op jit(solution)/shard_map/all_gather | solution.py:148
  104.5 1.6 fusion.53
  107.1 2.2 fusion.83
  110.3 2.4 broadcast_select_fusion.3
  112.8 6.4 %fusion.70 = f32[768,1024]{1,0:T(8,128)S(1)} fusion(bf16[4096,1536]{1,0:T(8,128)(2,1)} %all-gather.3.cloned.1.call-done, bf16[384,2048]{1,0:T(8,128)(2,1)S(1)} %get-tuple-element.253, bf16[384,2048]{1,0:T(8,128)(2,1)S(1)} %get-tuple-element.252), kind=kOutput, calls=%fused_computation.79 | convolution fusion | flops 3229089792 | bytes 10485760 | tf_op jit(solution)/shard_map/dot_general | solution.py:154
  119.2 2.0 fusion.92
  121.2 3.1 %reshape.138 = f32[768,2,256]{2,1,0:T(2,128)} reshape(f32[768,512]{1,0:T(8,128)} %get-tuple-element.251) | data formatting | bytes 3145728 | tf_op jit(solution)/shard_map/reshape | solution.py:162
  124.2 3.0 %reshape.139 = f32[768,2,256]{2,1,0:T(2,128)} reshape(f32[768,512]{1,0:T(8,128)} %get-tuple-element.250) | data formatting | bytes 3145728 | tf_op jit(solution)/shard_map/reshape | solution.py:161
  127.3 7.7 %fusion.73 = bf16[768,1024]{1,0:T(8,128)(2,1)} fusion(bf16[4096,1536]{1,0:T(8,128)(2,1)} %all-gather.3.cloned.1.call-done, bf16[384,2048]{1,0:T(8,128)(2,1)} %copy-done.7, bf16[384,2048]{1,0:T(8,128)(2,1)} %copy-done.6), kind=kOutput, calls=%fused_computation.80 | convolution fusion | flops 3228303360 | bytes 8912896 | tf_op jit(solution)/shard_map/dot_general | solution.py:154
  135.0 3.8 %reshape_reshape.3 = bf16[6,128,2,512]{3,2,1,0:T(2,128)(2,1)} reshape(bf16[768,1024]{1,0:T(8,128)(2,1)} %fusion.73) | data formatting | bytes 3145728 | tf_op jit(solution)/shard_map/reshape;reshape | solution.py:81
  138.8 3.0 %copy.58 = bf16[6,128,2,512]{3,1,2,0:T(8,128)(2,1)} copy(bf16[6,128,2,512]{3,2,1,0:T(2,128)(2,1)} %reshape_reshape.3) | data formatting | bytes 3145728 | tf_op jit(solution)/shard_map/reshape;reshape | solution.py:81
  145.4 30.5 %while.15 = (s32[]{:T(128)}, f32[2,256,512]{2,1,0:T(8,128)S(1)}, f32[6,2,128,512]{3,2,1,0:T(8,128)}, bf16[6,2,128,256]{3,2,0,1:T(8,128)(2,1)}, bf16[6,2,128,512]...) while((s32[]{:T(128)}, f32[2,256,512]{2,1,0:T(8,128)S(1)}, ...), condition=%wide.region_2.4_spmd.clone.clone.clone, body=%wide.region_1.3_spmd.clone.clone.clone.sunk | while | flops 186188304 | bytes 5857972 | solution.py:110
  145.5 1.2 convolution_multiply_fusion.3
  146.6 2.3 fusion.108
  148.9 1.5 convolution_add_fusion.3
  150.5 1.1 convolution_multiply_fusion.3
  151.7 2.3 fusion.108
  154.0 1.5 convolution_add_fusion.3
  155.6 1.1 convolution_multiply_fusion.3
  156.7 2.3 fusion.108
  159.0 1.5 convolution_add_fusion.3
  160.6 1.1 convolution_multiply_fusion.3
  161.8 2.4 fusion.108
  164.2 1.5 convolution_add_fusion.3
  167.0 2.3 fusion.108
  169.3 1.5 convolution_add_fusion.3
  170.9 1.2 convolution_multiply_fusion.3
  172.1 2.3 fusion.108
  174.4 1.5 convolution_add_fusion.3
  175.9 2.2 multiply_reduce_fusion
  178.3 1.2 mul.294
  181.4 2.4 copy.38
  185.4 3.6 %fusion.63 = f32[768,2048]{1,0:T(8,128)S(1)} fusion(bf16[4096,1536]{1,0:T(8,128)(2,1)} %all-gather.3.cloned.1.call-done, bf16[768,1024]{1,0:T(8,128)(2,1)S(1)} %multiply_convert_fusion.3), kind=kOutput, calls=%fused_computation.76 | convolution fusion | flops 1610612736 | bytes 9175040 | tf_op jit(solution)/shard_map/dot_general | solution.py:157
  189.0 3.5 %add_convert_fusion.1 = bf16[768,2048]{1,0:T(8,128)(2,1)S(1)} fusion(f32[768,2048]{1,0:T(8,128)S(1)} %fusion.63, bf16[4096,1536]{1,0:T(8,128)(2,1)} %all-gather.3.cloned.1.call-done, bf16[768,1024]{1,0:T(8,128)(2,1)S(1)} %multiply_convert_fusion.3), kind=kOutput, calls=%fused_computation.44 | convolution fusion | flops 1613758464 | bytes 12320768 | tf_op jit(solution)/shard_map/dot_general | solution.py:157
  192.5 1.6 copy-done.2
  194.7 3.2 %collective-permute-done.1 = bf16[384,2048]{1,0:T(8,128)(2,1)} collective-permute-done((bf16[384,2048]{1,0:T(8,128)(2,1)S(1)}, bf16[384,2048]{1,0:T(8,128)(2,1)}, u32[]{:S(2)}, u32[]{:S(2)}) %collective-permute-start.1) | collective-permute-done | bytes 1572896 | tf_op jit(solution)/shard_map/ppermute | solution.py:32
  197.9 3.0 %fusion.55 = (f32[384]{0:T(512)S(1)}, bf16[384,2048]{1,0:T(8,128)(2,1)S(1)}) fusion(bf16[384,2048]{1,0:T(8,128)(2,1)} %collective-permute-done.1, bf16[768,2048]{1,0:T(8,128)(2,1)} %copy-done.2, s32[]{:T(128)S(6)} %select_n.56, bf16[384,2048]{1,0:T(8,128)(2,1)S(1)} %copy-done), kind=kLoop, calls=%fused_computation.64 | loop fusion | flops 7077504 | bytes 6292996 | tf_op jit(solution)/shard_map/reduce_sum | solution.py:42
  201.8 3.1 %collective-permute-done.2 = bf16[384,2048]{1,0:T(8,128)(2,1)S(1)} collective-permute-done((bf16[384,2048]{1,0:T(8,128)(2,1)S(1)}, bf16[384,2048]{1,0:T(8,128)(2,1)S(1)}, u32[]{:S(2)}, u32[]{:S(2)}) %collective-permute-start.2) | collective-permute-done | bytes 1572896 | tf_op jit(solution)/shard_map/ppermute | solution.py:22
  204.9 2.2 broadcast_select_fusion.1
  207.1 6.4 %all-gather.5.cloned.1.call-done = bf16[4096,2112]{1,0:T(8,128)(2,1)} async-done(((bf16[64,2112]{1,0:T(8,128)(2,1)}), bf16[4096,2112]{1,0:T(8,128)(2,1)}) %all-gather.5.cloned.1.call-update) | async-done | bytes 17301520 | tf_op jit(solution)/shard_map/all_gather | solution.py:150
  213.5 9.7 %fusion.45 = f32[768,1408]{1,0:T(8,128)} fusion(bf16[4096,2112]{1,0:T(8,128)(2,1)} %all-gather.5.cloned.1.call-done, bf16[384,2048]{1,0:T(8,128)(2,1)} %get-tuple-element.249, bf16[384,2048]{1,0:T(8,128)(2,1)S(1)} %get-tuple-element.248), kind=kOutput, calls=%fused_computation.47 | convolution fusion | flops 4435476480 | bytes 13238272 | tf_op jit(solution)/shard_map/dot_general | solution.py:154
  223.4 7.9 %multiply_convert_fusion.2 = bf16[768,1408]{1,0:T(8,128)(2,1)S(1)} fusion(f32[768,1408]{1,0:T(8,128)} %fusion.45, bf16[4096,2112]{1,0:T(8,128)(2,1)S(1)} %copy-done.12, bf16[384,2048]{1,0:T(8,128)(2,1)S(1)} %copy-done.8, bf16[384,2048]{1,0:T(8,128)(2,1)S(1)} %get-tuple-element.248), kind=kOutput, calls=%fused_computation.55 | convolution fusion | flops 4441964544 | bytes 15400960 | tf_op jit(solution)/shard_map/dot_general | solution.py:154
  231.2 4.6 %fusion.60 = f32[768,2048]{1,0:T(8,128)} fusion(bf16[4096,2112]{1,0:T(8,128)(2,1)S(1)} %copy-done.12, bf16[768,1408]{1,0:T(8,128)(2,1)S(1)} %multiply_convert_fusion.2), kind=kOutput, calls=%fused_computation.69 | convolution fusion | flops 2214592512 | bytes 10616832 | tf_op jit(solution)/shard_map/dot_general | solution.py:157
  235.9 4.8 %add_convert_fusion = bf16[768,2048]{1,0:T(8,128)(2,1)S(1)} fusion(f32[768,2048]{1,0:T(8,128)} %fusion.60, bf16[4096,2112]{1,0:T(8,128)(2,1)S(1)} %copy-done.12, bf16[768,1408]{1,0:T(8,128)(2,1)S(1)} %multiply_convert_fusion.2), kind=kOutput, calls=%fused_computation.43 | convolution fusion | flops 2217738240 | bytes 13762560 | tf_op jit(solution)/shard_map/dot_general | solution.py:157
  241.7 3.0 %collective-permute-done.3 = bf16[384,2048]{1,0:T(8,128)(2,1)S(1)} collective-permute-done((bf16[384,2048]{1,0:T(8,128)(2,1)S(1)}, bf16[384,2048]{1,0:T(8,128)(2,1)S(1)}, u32[]{:S(2)}, u32[]{:S(2)}) %collective-permute-start.3) | collective-permute-done | bytes 1572896 | tf_op jit(solution)/shard_map/ppermute | solution.py:32
  244.8 2.0 fusion.58
  (72 shorter events, 16.1 us)
Async XLA Ops:
  6.5 97.6 %copy-start = (bf16[384,2048]{1,0:T(8,128)(2,1)S(1)}, bf16[384,2048]{1,0:T(8,128)(2,1)}, u32[]{:S(2)}) copy-start(bf16[384,2048]{1,0:T(8,128)(2,1)} %param.15) | copy-start | bytes 4718596
  6.5 98.0 %copy-start.9 = (f32[2048]{0:T(1024)S(1)}, f32[2048]{0:T(1024)}, u32[]{:S(2)}) copy-start(f32[2048]{0:T(1024)} %param.16) | copy-start | bytes 24580
  6.5 97.5 %all-gather.3.cloned.1.call-start = ((), (), s32[]{:S(2)}) async-start(), calls=%async_computation | async-start | bytes 12779520 | tf_op jit(solution)/shard_map/all_gather | solution.py:148
  9.3 204.2 %all-gather.5.cloned.1.call-start = ((), (), s32[]{:S(2)}) async-start(), calls=%async_computation.1 | async-start | bytes 18104320 | tf_op jit(solution)/shard_map/all_gather | solution.py:150
  106.1 4.2 %collective-permute-start = (bf16[384,2048]{1,0:T(8,128)(2,1)}, bf16[384,2048]{1,0:T(8,128)(2,1)}, u32[]{:S(2)}, u32[]{:S(2)}) collective-permute-start(bf16[384,2048]{1,0:T(8,128)(2,1)} %fusion.53), channel_id=1, source_target_pairs={{0,1},{1,0},{2,3},{3,2},{4,5},{5,4},{6,7},{7,6},{8,9},{9,8},{10,11... | collective-permute-start | bytes 4718600 | tf_op jit(solution)/shard_map/ppermute | solution.py:22
  112.8 6.4 %copy-start.6 = (bf16[384,2048]{1,0:T(8,128)(2,1)}, bf16[384,2048]{1,0:T(8,128)(2,1)S(1)}, u32[]{:S(2)}) copy-start(bf16[384,2048]{1,0:T(8,128)(2,1)S(1)} %get-tuple-element.252) | copy-start | bytes 4718596
  112.8 6.4 %copy-start.7 = (bf16[384,2048]{1,0:T(8,128)(2,1)}, bf16[384,2048]{1,0:T(8,128)(2,1)S(1)}, u32[]{:S(2)}) copy-start(bf16[384,2048]{1,0:T(8,128)(2,1)S(1)} %get-tuple-element.253) | copy-start | bytes 4718596
  138.8 3.0 %copy-start.3 = (f32[768,2,256]{2,1,0:T(2,128)S(1)}, f32[768,2,256]{2,1,0:T(2,128)}, u32[]{:S(2)}) copy-start(f32[768,2,256]{2,1,0:T(2,128)} %reshape.138) | copy-start | bytes 4718596
  138.8 3.0 %copy-start.4 = (f32[768,2,256]{2,1,0:T(2,128)S(1)}, f32[768,2,256]{2,1,0:T(2,128)}, u32[]{:S(2)}) copy-start(f32[768,2,256]{2,1,0:T(2,128)} %reshape.139) | copy-start | bytes 4718596
  141.8 1.1 copy-start.5
  179.5 1.9 copy-start.1
  183.9 0.8 copy-start.11
  192.5 1.6 copy-start.2
  194.2 3.7 %collective-permute-start.1 = (bf16[384,2048]{1,0:T(8,128)(2,1)S(1)}, bf16[384,2048]{1,0:T(8,128)(2,1)}, u32[]{:S(2)}, u32[]{:S(2)}) collective-permute-start(bf16[384,2048]{1,0:T(8,128)(2,1)S(1)} %constant_dynamic-slice_fusion.1), channel_id=1, source_target_pairs={{0,1},{1,0},{2,3},{3,2},{4,5},{5,4},{6,7},{7,6},{8,9},{9,8},{10,11... | collective-permute-start | bytes 4718600 | tf_op jit(solution)/shard_map/ppermute | solution.py:32
  194.7 6.2 %copy-start.10 = (f32[2048]{0:T(1024)S(1)}, f32[2048]{0:T(1024)}, u32[]{:S(2)}) copy-start(f32[2048]{0:T(1024)} %param.22) | copy-start | bytes 24580
  201.4 3.5 %collective-permute-start.2 = (bf16[384,2048]{1,0:T(8,128)(2,1)S(1)}, bf16[384,2048]{1,0:T(8,128)(2,1)S(1)}, u32[]{:S(2)}, u32[]{:S(2)}) collective-permute-start(bf16[384,2048]{1,0:T(8,128)(2,1)S(1)} %fusion.57), channel_id=1, source_target_pairs={{0,1},{1,0},{2,3},{3,2},{4,5},{5,4},{6,7},{7,6},{8,9},{9,8},{10,11... | collective-permute-start | bytes 4718600 | tf_op jit(solution)/shard_map/ppermute | solution.py:22
  213.5 9.7 %copy-start.8 = (bf16[384,2048]{1,0:T(8,128)(2,1)S(1)}, bf16[384,2048]{1,0:T(8,128)(2,1)}, u32[]{:S(2)}) copy-start(bf16[384,2048]{1,0:T(8,128)(2,1)} %get-tuple-element.249) | copy-start | bytes 4718596
  213.5 9.9 %copy-start.12 = (bf16[4096,2112]{1,0:T(8,128)(2,1)S(1)}, bf16[4096,2112]{1,0:T(8,128)(2,1)}, u32[]{:S(2)}) copy-start(bf16[4096,2112]{1,0:T(8,128)(2,1)} %all-gather.5.cloned.1.call-done) | copy-start | bytes 51904516
  240.8 3.9 %collective-permute-start.3 = (bf16[384,2048]{1,0:T(8,128)(2,1)S(1)}, bf16[384,2048]{1,0:T(8,128)(2,1)S(1)}, u32[]{:S(2)}, u32[]{:S(2)}) collective-permute-start(bf16[384,2048]{1,0:T(8,128)(2,1)S(1)} %constant_dynamic-slice_fusion), channel_id=1, source_target_pairs={{0,1},{1,0},{2,3},{3,2},{4,5},{5,4},{6,7},{7,6},{8,9},{9,8},{10,11... | collective-permute-start | bytes 4718600 | tf_op jit(solution)/shard_map/ppermute | solution.py:32
Sparse Core Ops, SparseCore 0:
  10.1 93.9 all-gather.2
  106.9 106.5 all-gather.4
